TPU v7x, 32 devices: a whole 2x2x4 slice. The times are simulated.
32 devices in a mesh: grp: 2 (over y), fs: 4 (over z), tp: 4 (over x, core).
Axes of the slice: x: 2, y: 2, z: 4, core: 2. Of those that a mesh axis runs over, the one named last changes fastest.
Arguments:
- tokens: bfloat16 [2048, 2048], P(('grp', 'fs')), parts along dimension 0, may hold values from -6 to 6
- route_ids: int32 [2048, 2], P(('grp', 'fs')), parts along dimension 0, may hold values from 0 to 7, as said below
- route_weights: float32 [2048, 2], P(('grp', 'fs')), parts along dimension 0, may hold values from 0.2 to 1
- ffn_gain: float32 [2048], P('fs'), may hold values from 0.1 to 1.9
- gate_master: float32 [8, 2048, 1024], P(None, 'fs', 'tp'), may hold values from -0.125 to 0.125
- up_master: float32 [8, 2048, 1024], P(None, 'fs', 'tp'), may hold values from -0.125 to 0.125
- down_master: float32 [8, 1024, 2048], P(None, 'fs', 'tp'), may hold values from -0.1875 to 0.1875
Outputs:
- gate_serve: bfloat16 [16, 2048, 1024], P(('grp', 'fs'), None, 'tp'), parts along dimension 0
- up_serve: bfloat16 [16, 2048, 1024], P(('grp', 'fs'), None, 'tp'), parts along dimension 0
- down_serve: bfloat16 [16, 1024, 2048], P(('grp', 'fs'), None, 'tp'), parts along dimension 0
- mixed: bfloat16 [2048, 2048], P(('grp', 'fs'), 'tp'), parts along dimension 0
There are 2 independent parts, one for each index of `grp`. A program takes and returns all parts, laid end to end along the dimension named above; an argument that names none is the same for every part. Nothing has to cross between parts.
Inputs may be any that keep to these rules, and one draw needn't show every extreme that they name: `route_ids`: each row names two different experts of one group of 8 consecutive experts. Among the tokens of one index of fs, each group is named by exactly 256 tokens and no expert by more than 128; in every group one expert, the same for every index of fs, is named by exactly 128, and so is one other expert of the group, which may change from one index of fs to the next.
All inputs are finite; a program needn't handle non-finite values.
Results may differ from a plain program's by a relative error of at most 0.0087.
Values may be sent and summed in bfloat16 or wider, within the bound.
A program may use at most 64 MiB of HBM per device.

v0:
```python
import jax
import jax.numpy as jnp
from jax import lax
from jax.sharding import PartitionSpec as P

GROUP_SIZE = 8


def slot_targets(route_ids, experts, capacity):
    flat_ids = route_ids.reshape(-1)
    member = (flat_ids[:, None] == jnp.arange(experts, dtype=jnp.int32)[None, :]).astype(jnp.int32)
    before = jnp.cumsum(member, axis=0) - member
    slot_index = jnp.sum(before * member, axis=1)
    return flat_ids * capacity + slot_index


def fill_slots(source, targets, experts, capacity):
    doubled = jnp.repeat(source, 2, axis=0)
    buffer = jnp.zeros((experts * capacity, source.shape[1]), source.dtype).at[targets].set(doubled)
    return buffer.reshape(experts, capacity, source.shape[1])


def on_device(tokens, route_ids, route_weights, ffn_gain, gate_master, up_master, down_master):
    row_gain = ffn_gain[None, :, None]
    gate_local = (gate_master * row_gain).astype(jnp.bfloat16)
    up_local = (up_master * row_gain).astype(jnp.bfloat16)
    down_local = down_master.astype(jnp.bfloat16)
    gate_serve, up_serve, down_serve = (
        lax.all_to_all(gate_local, "fs", split_axis=0, concat_axis=1, tiled=True),
        lax.all_to_all(up_local, "fs", split_axis=0, concat_axis=1, tiled=True),
        lax.all_to_all(down_local, "fs", split_axis=0, concat_axis=1, tiled=True),
    )
    experts = gate_local.shape[0]
    capacity = tokens.shape[0] // (2 * (experts // GROUP_SIZE))
    token_rows = tokens.astype(jnp.float32)
    normed = (
        token_rows * lax.rsqrt(jnp.mean(token_rows * token_rows, axis=1, keepdims=True) + 1e-06)
    ).astype(jnp.bfloat16)
    targets = slot_targets(route_ids, experts, capacity)
    col_width = normed.shape[1] // lax.axis_size("tp")
    own_cols = lax.dynamic_slice_in_dim(normed, lax.axis_index("tp") * col_width, col_width, 1)
    part_rows = lax.all_to_all(
        fill_slots(own_cols, targets, experts, capacity),
        "fs",
        split_axis=0,
        concat_axis=1,
        tiled=True,
    )
    portion = lax.all_gather(part_rows, "tp", axis=2, tiled=True)
    gate_part = jnp.einsum("erd,edf->erf", portion, gate_serve, preferred_element_type=jnp.float32)
    up_part = jnp.einsum("erd,edf->erf", portion, up_serve, preferred_element_type=jnp.float32)
    hidden = (jax.nn.silu(gate_part) * up_part).astype(jnp.bfloat16)
    expert_out = jnp.einsum(
        "erf,efd->erd",
        lax.all_gather(hidden, "tp", axis=2, tiled=True),
        down_serve,
        preferred_element_type=jnp.float32,
    ).astype(jnp.bfloat16)
    returned_rows = lax.all_to_all(expert_out, "fs", split_axis=1, concat_axis=0, tiled=True)
    picked = returned_rows.reshape(-1, returned_rows.shape[2])[targets].astype(jnp.float32)
    weighted = picked * route_weights.reshape(-1, 1)
    combined = jnp.sum(weighted.reshape(-1, 2, returned_rows.shape[2]), axis=1).astype(jnp.bfloat16)
    return (gate_serve, up_serve, down_serve, combined)


def solution(mesh):
    in_specs = (
        P(("grp", "fs"), None),
        P(("grp", "fs"), None),
        P(("grp", "fs"), None),
        P("fs"),
        P(None, "fs", "tp"),
        P(None, "fs", "tp"),
        P(None, "fs", "tp"),
    )
    out_specs = (
        P(("grp", "fs"), None, "tp"),
        P(("grp", "fs"), None, "tp"),
        P(("grp", "fs"), None, "tp"),
        P(("grp", "fs"), "tp"),
    )
    return jax.shard_map(
        on_device, mesh=mesh, in_specs=in_specs, out_specs=out_specs, check_vma=False
    )
```

profile of v0, /device:TPU:0, one launch (start us, length us, event | category | flops | bytes accessed | tf_op | source)
XLA Modules:
  0.0 250.0 jit_solution(12472034540438758420)
XLA Ops:
  7.2 1.5 convert_element_type.43
  11.9 3.5 %scatter_custom_fusion = bf16[1024,512]{1,0:T(8,128)(2,1)} fusion(s32[512]{0:T(512)S(1)} %bitcast.49, bf16[512,512]{1,0:T(8,128)(2,1)S(1)} %reshape.101, bf16[]{:T(256)} %constant.11.clone.1), kind=kCustom, calls=%fused_computation.11 | custom fusion | bytes 1048578 | tf_op jit(solution)/shard_map/scatter | solution.py:19
  15.4 6.3 %all-to-all-start.3 = ((bf16[8,128,512]{2,1,0:T(8,128)(2,1)}), bf16[8,128,512]{2,1,0:T(8,128)(2,1)S(1)}, u32[]{:S(2)}, u32[]{:S(2)}) async-start(bf16[8,128,512]{2,1,0:T(8,128)(2,1)} %bitcast.13), calls=%async_computation.3 | async-start | bytes 2097152 | tf_op jit(solution)/shard_map/all_to_all | solution.py:42
  21.7 6.5 %multiply_convert_fusion = (bf16[8,512,256]{2,1,0:T(8,128)(2,1)}, bf16[8,512,256]{2,1,0:T(8,128)(2,1)}) fusion(f32[8,512,256]{2,1,0:T(8,128)} %param.12, f32[512]{0:T(512)S(1)} %copy-done.4, f32[8,512,256]{2,1,0:T(8,128)} %param.11), kind=kLoop, calls=%fused_computation.2 | loop fusion | flops 4194304 | bytes 12584960 | tf_op jit(solution)/shard_map/convert_element_type | solution.py:26
  28.2 19.3 %all-to-all-done.3 = bf16[8,128,512]{2,1,0:T(8,128)(2,1)S(1)} async-done(((bf16[8,128,512]{2,1,0:T(8,128)(2,1)}), bf16[8,128,512]{2,1,0:T(8,128)(2,1)S(1)}, u32[]{:S(2)}, u32[]{:S(2)}) %all-to-all-start.3) | async-done | bytes 1048608 | tf_op jit(solution)/shard_map/all_to_all | solution.py:42
  47.5 3.6 %all-to-all-start = ((bf16[8,512,256]{2,1,0:T(8,128)(2,1)}), bf16[8,512,256]{2,1,0:T(8,128)(2,1)S(1)}, u32[]{:S(2)}, u32[]{:S(2)}) async-start(bf16[8,512,256]{2,1,0:T(8,128)(2,1)} %get-tuple-element.5), calls=%async_computation | async-start | bytes 4194304 | tf_op jit(solution)/shard_map/all_to_all | solution.py:29
  51.1 1.2 copy.31
  52.3 46.5 %all-to-all-done = bf16[8,512,256]{2,1,0:T(8,128)(2,1)S(1)} async-done(((bf16[8,512,256]{2,1,0:T(8,128)(2,1)}), bf16[8,512,256]{2,1,0:T(8,128)(2,1)S(1)}, u32[]{:S(2)}, u32[]{:S(2)}) %all-to-all-start) | async-done | bytes 2097184 | tf_op jit(solution)/shard_map/all_to_all | solution.py:29
  98.8 4.5 %all-to-all-start.1 = ((bf16[8,512,256]{2,1,0:T(8,128)(2,1)}), bf16[8,512,256]{2,1,0:T(8,128)(2,1)}, u32[]{:S(2)}, u32[]{:S(2)}) async-start(bf16[8,512,256]{2,1,0:T(8,128)(2,1)} %get-tuple-element.4), calls=%async_computation.1 | async-start | bytes 4194304 | tf_op jit(solution)/shard_map/all_to_all | solution.py:30
  103.3 3.8 %convert_element_type.40 = bf16[8,256,512]{2,1,0:T(8,128)(2,1)} convert(f32[8,256,512]{2,1,0:T(8,128)} %param.13) | non-fusion elementwise | flops 1048576 | bytes 6291456 | tf_op jit(solution)/shard_map/convert_element_type | solution.py:27
  107.0 1.5 copy.25
  108.5 42.6 %all-to-all-done.1 = bf16[8,512,256]{2,1,0:T(8,128)(2,1)} async-done(((bf16[8,512,256]{2,1,0:T(8,128)(2,1)}), bf16[8,512,256]{2,1,0:T(8,128)(2,1)}, u32[]{:S(2)}, u32[]{:S(2)}) %all-to-all-start.1) | async-done | bytes 2097184 | tf_op jit(solution)/shard_map/all_to_all | solution.py:30
  151.1 3.6 %all-to-all-start.2 = ((bf16[8,256,512]{2,1,0:T(8,128)(2,1)}), bf16[8,256,512]{2,1,0:T(8,128)(2,1)S(1)}, u32[]{:S(2)}, u32[]{:S(2)}) async-start(bf16[8,256,512]{2,1,0:T(8,128)(2,1)} %convert_element_type.40), calls=%async_computation.2 | async-start | bytes 4194304 | tf_op jit(solution)/shard_map/all_to_all | solution.py:31
  154.7 3.0 %copy.26 = bf16[4,2,512,256]{3,2,0,1:T(8,128)(2,1)} copy(bf16[4,2,512,256]{3,2,1,0:T(8,128)(2,1)} %bitcast.3) | data formatting | bytes 4194304 | tf_op jit(solution)/shard_map/all_to_all | solution.py:30
  157.8 4.2 %fusion.7 = f32[2,512,256]{2,1,0:T(8,128)S(1)} fusion(bf16[2,512,2048]{2,1,0:T(8,128)(2,1)} %all-gather.3.cloned.1.call-done, bf16[2,2048,256]{2,1,0:T(8,128)(2,1)} %bitcast.43), kind=kOutput, calls=%fused_computation.24 | convolution fusion | flops 1073741824 | bytes 7340032 | tf_op jit(solution)/shard_map/erd,edf->erf/dot_general | solution.py:50
  162.5 2.1 fusion
  164.6 37.8 %all-to-all-done.2 = bf16[8,256,512]{2,1,0:T(8,128)(2,1)S(1)} async-done(((bf16[8,256,512]{2,1,0:T(8,128)(2,1)}), bf16[8,256,512]{2,1,0:T(8,128)(2,1)S(1)}, u32[]{:S(2)}, u32[]{:S(2)}) %all-to-all-start.2) | async-done | bytes 2097184 | tf_op jit(solution)/shard_map/all_to_all | solution.py:31
  202.4 1.5 copy.27
  204.0 3.5 %convolution_convert_fusion = bf16[2,512,512]{2,1,0:T(8,128)(2,1)S(1)} fusion(bf16[2,512,1024]{2,1,0:T(8,128)(2,1)} %all-gather.5.cloned.1.call-done, bf16[2,1024,512]{2,1,0:T(8,128)(2,1)} %bitcast.47), kind=kOutput, calls=%fused_computation.5 | convolution fusion | flops 1074266112 | bytes 5242880 | tf_op jit(solution)/shard_map/erf,efd->erd/dot_general | solution.py:53
  207.4 2.0 copy.32
  209.5 3.7 %all-to-all-start.4 = ((bf16[2,512,512]{2,0,1:T(2,128)(2,1)}), bf16[2,512,512]{2,0,1:T(2,128)(2,1)S(1)}, u32[]{:S(2)}, u32[]{:S(2)}) async-start(bf16[2,512,512]{2,0,1:T(2,128)(2,1)} %copy.32), calls=%async_computation.4 | async-start | bytes 2097152 | tf_op jit(solution)/shard_map/all_to_all | solution.py:59
  213.4 24.9 %all-to-all-done.4 = bf16[2,512,512]{2,0,1:T(2,128)(2,1)S(1)} async-done(((bf16[2,512,512]{2,0,1:T(2,128)(2,1)}), bf16[2,512,512]{2,0,1:T(2,128)(2,1)S(1)}, u32[]{:S(2)}, u32[]{:S(2)}) %all-to-all-start.4) | async-done | bytes 1048608 | tf_op jit(solution)/shard_map/all_to_all | solution.py:59
  238.4 2.0 gather_fusion
  241.1 2.1 multiply_reduce_fusion.1
  (40 shorter events, 4.6 us)
Async XLA Ops:
  7.2 1.6 copy-start
  7.2 1.9 copy-start.2
  9.9 11.8 %copy-start.4 = (f32[512]{0:T(512)S(1)}, f32[512]{0:T(512)}, u32[]{:S(2)}) copy-start(f32[512]{0:T(512)} %param.10) | copy-start | bytes 6148
  15.4 32.1 %all-to-all-start.3 = ((bf16[8,128,512]{2,1,0:T(8,128)(2,1)}), bf16[8,128,512]{2,1,0:T(8,128)(2,1)S(1)}, u32[]{:S(2)}, u32[]{:S(2)}) async-start(bf16[8,128,512]{2,1,0:T(8,128)(2,1)} %bitcast.13), calls=%async_computation.3 | async-start | bytes 2097152 | tf_op jit(solution)/shard_map/all_to_all | solution.py:42
  47.5 51.3 %all-to-all-start = ((bf16[8,512,256]{2,1,0:T(8,128)(2,1)}), bf16[8,512,256]{2,1,0:T(8,128)(2,1)S(1)}, u32[]{:S(2)}, u32[]{:S(2)}) async-start(bf16[8,512,256]{2,1,0:T(8,128)(2,1)} %get-tuple-element.5), calls=%async_computation | async-start | bytes 4194304 | tf_op jit(solution)/shard_map/all_to_all | solution.py:29
  51.1 106.7 %all-gather.3.cloned.1.call-start = ((), (), s32[]{:S(2)}) async-start(), calls=%async_computation.5 | async-start | bytes 5242880 | tf_op jit(solution)/shard_map/all_gather | solution.py:49
  98.8 52.3 %all-to-all-start.1 = ((bf16[8,512,256]{2,1,0:T(8,128)(2,1)}), bf16[8,512,256]{2,1,0:T(8,128)(2,1)}, u32[]{:S(2)}, u32[]{:S(2)}) async-start(bf16[8,512,256]{2,1,0:T(8,128)(2,1)} %get-tuple-element.4), calls=%async_computation.1 | async-start | bytes 4194304 | tf_op jit(solution)/shard_map/all_to_all | solution.py:30
  151.1 51.3 %all-to-all-start.2 = ((bf16[8,256,512]{2,1,0:T(8,128)(2,1)}), bf16[8,256,512]{2,1,0:T(8,128)(2,1)S(1)}, u32[]{:S(2)}, u32[]{:S(2)}) async-start(bf16[8,256,512]{2,1,0:T(8,128)(2,1)} %convert_element_type.40), calls=%async_computation.2 | async-start | bytes 4194304 | tf_op jit(solution)/shard_map/all_to_all | solution.py:31
  154.7 49.3 %all-gather.5.cloned.1.call-start = ((), (), s32[]{:S(2)}) async-start(), calls=%async_computation.6 | async-start | bytes 2621440 | tf_op jit(solution)/shard_map/all_gather | solution.py:55
  157.8 4.3 %copy-start.1 = (bf16[4,2,512,256]{3,2,0,1:T(8,128)(2,1)S(1)}, bf16[4,2,512,256]{3,2,0,1:T(8,128)(2,1)}, u32[]{:S(2)}) copy-start(bf16[4,2,512,256]{3,2,0,1:T(8,128)(2,1)} %copy.26) | copy-start | bytes 6291460
  157.8 4.7 %copy-start.5 = (bf16[2,512,2048]{2,1,0:T(8,128)(2,1)S(1)}, bf16[2,512,2048]{2,1,0:T(8,128)(2,1)}, u32[]{:S(2)}) copy-start(bf16[2,512,2048]{2,1,0:T(8,128)(2,1)} %all-gather.3.cloned.1.call-done) | copy-start | bytes 12582916
  207.4 5.8 %copy-start.3 = (f32[256,2]{0,1:T(2,128)S(1)}, f32[256,2]{0,1:T(2,128)}, u32[]{:S(2)}) copy-start(f32[256,2]{0,1:T(2,128)} %param.9) | copy-start | bytes 6148
  209.5 28.8 %all-to-all-start.4 = ((bf16[2,512,512]{2,0,1:T(2,128)(2,1)}), bf16[2,512,512]{2,0,1:T(2,128)(2,1)S(1)}, u32[]{:S(2)}, u32[]{:S(2)}) async-start(bf16[2,512,512]{2,0,1:T(2,128)(2,1)} %copy.32), calls=%async_computation.4 | async-start | bytes 2097152 | tf_op jit(solution)/shard_map/all_to_all | solution.py:59
Sparse Core Ops, SparseCore 0:
  53.5 35.8 all-gather.2
  164.8 24.1 all-gather.4
where the time goes:
time: 251 us; the launch traced here: 250 us
  waiting for transfers between devices  171 us (68%)
  starting transfers between devices  21.8 us (9%)
  local copies, waits for them, and re-layouts  17.5 us (7%)
  other arithmetic  15.5 us (6%)
  between operations  14.3 us (6%)
  matrix products  9.85 us (4%)
    all_to_all x1, waiting for transfers between devices, on_device(): lax.all_to_all(gate_local, 'fs', split_axis=0, concat_axis=1, tiled=True)  46.5 us
    all_to_all x1, waiting for transfers between devices, on_device(): lax.all_to_all(up_local, 'fs', split_axis=0, concat_axis=1, tiled=True)  42.6 us
    all_to_all x1, waiting for transfers between devices, on_device(): lax.all_to_all(down_local, 'fs', split_axis=0, concat_axis=1, tiled=True)  37.8 us
    all_to_all x1, waiting for transfers between devices, on_device(): lax.all_to_all(expert_out, 'fs', split_axis=1, concat_axis=0, tiled=True)  24.9 us
    all_to_all x1, waiting for transfers between devices, on_device(): lax.all_to_all(fill_slots(own_cols, targets, experts, capacity), 'fs', sp...  19.3 us
    convert_element_type x1, other arithmetic, on_device(): up_local = (up_master * row_gain).astype(jnp.bfloat16)  6.46 us
    all_to_all x1, starting transfers between devices, on_device(): lax.all_to_all(fill_slots(own_cols, targets, experts, capacity), 'fs', sp...  6.35 us
  transfers between devices with their start and end apart: 7, of which 5 were waited for; matrix products, arithmetic and copies ran while one was open for 10% of the time, Pallas kernels for 0%

commit v1 on v0

v1 whole, which is shorter than its diff:
```python
import functools

import jax
import jax.numpy as jnp
from jax import lax
from jax.experimental import pallas as pl
from jax.experimental.pallas import tpu as pltpu
from jax.sharding import PartitionSpec as P

GROUP_SIZE = 8
MESH = pl.DeviceIdType.MESH


def slot_targets(route_ids, experts, capacity):
    flat_ids = route_ids.reshape(-1)
    member = (flat_ids[:, None] == jnp.arange(experts, dtype=jnp.int32)[None, :]).astype(jnp.int32)
    before = jnp.cumsum(member, axis=0) - member
    slot_index = jnp.sum(before * member, axis=1)
    return flat_ids * capacity + slot_index


def kernel(
    G, N, T, cap,
    tok_ref, meta_ref, gain_ref, gate_hbm, up_hbm, down_hbm,
    gs_ref, us_ref, ds_ref, mixed_ref,
    gate_f, up_f, down_f, stage_gu, stage_d, tok_all, meta_all, x_buf, hid_all, part_send, part_recv,
    load_sem, ts, tr, ms, mr, xs, xr, zs, zr, ys, yr, hs, hr, ps, pr,
):
    g, z, t = lax.axis_index("grp"), lax.axis_index("fs"), lax.axis_index("tp")
    E, R, C = gate_f.shape
    Ed = E // N
    tokens, Dq = tok_ref.shape[1:]
    FFq = C
    masters, serves = (gate_f, up_f, down_f), (gs_ref, us_ref, ds_ref)
    rows = (R, R, down_f.shape[1])

    loads = [
        pltpu.make_async_copy(src, dst, load_sem.at[w])
        for w, (src, dst) in enumerate(zip((gate_hbm, up_hbm, down_hbm), masters))
    ]
    for load in loads:
        load.start()

    barrier = pltpu.get_barrier_semaphore()
    for axis, me, size in (("grp", g, G), ("fs", z, N), ("tp", t, T)):
        for k in range(1, size):
            pl.semaphore_signal(barrier, inc=1, device_id={axis: lax.rem(me + k, size)}, device_id_type=MESH)
    pl.semaphore_wait(barrier, G + N + T - 3)

    def remote(src, dst, send, recv, axis, peer):
        copy = pltpu.make_async_remote_copy(
            src_ref=src, dst_ref=dst, send_sem=send, recv_sem=recv, device_id={axis: peer}, device_id_type=MESH
        )
        copy.start()
        return copy

    sent = []
    tok_copies, meta_copies = {}, {}
    for k in range(1, N):
        peer = lax.rem(z + k, N)
        meta_copies[k] = remote(meta_ref, meta_all.at[z], ms.at[k], mr.at[k], "fs", peer)
        tok_copies[k] = remote(tok_ref.at[t], tok_all.at[z, t], ts.at[k], tr.at[k], "fs", peer)

    z_copies = {}

    def send_weights(w):
        loads[w].wait()
        sub = rows[w] // G
        start = pl.multiple_of(g * sub, sub)
        for k in range(1, N):
            peer = lax.rem(z + k, N)
            stage = stage_d.at[k] if w == 2 else stage_gu.at[w, k]
            for e in range(Ed):
                block = masters[w][peer * Ed + e, pl.ds(start, sub), :]
                if w < 2:
                    block = block * gain_ref[pl.ds(start, sub), :]
                stage[e] = block.astype(jnp.bfloat16)
            where = pl.multiple_of(z * rows[w] + start, sub)
            z_copies[w, k] = remote(
                stage, serves[w].at[:, pl.ds(where, sub), :], zs.at[w, k], zr.at[w, k], "fs", peer
            )

    def keep_own(w):
        where = pl.multiple_of(z * rows[w], rows[w])
        for e in range(Ed):
            block = masters[w][z * Ed + e]
            if w < 2:
                block = block * gain_ref[...]
            serves[w][e, pl.ds(where, rows[w]), :] = block.astype(jnp.bfloat16)

    y_copies = []

    def relay_weights(w):
        sub = rows[w] // G
        for k in range(1, N):
            z_copies[w, k].wait_recv()
            origin = lax.rem(z + N - k, N)
            where = pl.multiple_of(origin * rows[w] + g * sub, sub)
            view = serves[w].at[:, pl.ds(where, sub), :]
            for j in range(1, G):
                y_copies.append(
                    (w, remote(view, view, ys.at[w, k, j], yr.at[w, k, j], "grp", lax.rem(g + j, G)))
                )

    def finish_weights(w):
        for which, copy in y_copies:
            if which == w:
                copy.wait_recv()

    send_weights(0)
    send_weights(1)
    send_weights(2)

    meta_all[z] = meta_ref[...]
    tok_all[z] = tok_ref[...]
    for w in range(3):
        keep_own(w)

    x_copies = []
    for k in range(1, N):
        tok_copies[k].wait_recv()
        origin = lax.rem(z + N - k, N)
        view = tok_all.at[origin, t]
        for j in range(1, T):
            x_copies.append(remote(view, view, xs.at[k, j], xr.at[k, j], "tp", lax.rem(t + j, T)))
    for k in range(1, N):
        meta_copies[k].wait_recv()
    relay_weights(0)
    for copy in x_copies:
        copy.wait_recv()

    SB = Ed * cap
    base = (z * SB).astype(jnp.float32)

    def hits(n):
        slot = lax.broadcasted_iota(jnp.int32, (SB, tokens), 0).astype(jnp.float32) + base
        info = meta_all[n]
        return info[0:1, :] == slot, info[1:2, :] == slot, info

    def dispatch(n, carry):
        first, second, _ = hits(n)
        pick = (first.astype(jnp.float32) + second.astype(jnp.float32)).astype(jnp.bfloat16)
        for q in range(T):
            got = jnp.dot(pick, tok_all[n, q], preferred_element_type=jnp.float32).astype(jnp.bfloat16)
            for e in range(Ed):
                x_buf[e, pl.ds(pl.multiple_of(n * cap, cap), cap), q * Dq:(q + 1) * Dq] = got[e * cap:(e + 1) * cap]
        return carry

    lax.fori_loop(0, N, dispatch, 0)
    relay_weights(1)
    finish_weights(0)
    finish_weights(1)

    def experts_in(i, carry):
        e = i // N
        at = pl.ds(pl.multiple_of((i % N) * cap, cap), cap)
        x = x_buf[e, at, :]
        gate = jnp.dot(x, gs_ref[e], preferred_element_type=jnp.float32)
        up = jnp.dot(x, us_ref[e], preferred_element_type=jnp.float32)
        hid_all[t, e, at, :] = (gate / (1.0 + jnp.exp(-gate)) * up).astype(jnp.bfloat16)
        return carry

    lax.fori_loop(0, Ed * N, experts_in, 0)
    h_copies = []
    for j in range(1, T):
        view = hid_all.at[t]
        h_copies.append(remote(view, view, hs.at[j], hr.at[j], "tp", lax.rem(t + j, T)))
    relay_weights(2)
    finish_weights(2)
    for copy in h_copies:
        copy.wait_recv()

    def partial_rows(n):
        first, second, info = hits(n)
        weight = jnp.sum(
            jnp.where(first, info[2:3, :], 0.0) + jnp.where(second, info[3:4, :], 0.0), axis=1, keepdims=True
        )
        pick = (first.astype(jnp.float32) + second.astype(jnp.float32)).astype(jnp.bfloat16)
        at = pl.ds(pl.multiple_of(n * cap, cap), cap)
        outs = []
        for e in range(Ed):
            out = jnp.zeros((cap, ds_ref.shape[2]), jnp.float32)
            for q in range(T):
                out += jnp.dot(
                    hid_all[q, e, at, :], ds_ref[e, q * FFq:(q + 1) * FFq, :], preferred_element_type=jnp.float32
                )
            outs.append(out.astype(jnp.bfloat16).astype(jnp.float32))
        scaled = (jnp.concatenate(outs, axis=0) * weight).astype(jnp.bfloat16)
        return lax.dot_general(pick, scaled, (((0,), (0,)), ((), ())), preferred_element_type=jnp.float32)

    p_copies = []
    for k in range(1, N):
        peer = lax.rem(z + k, N)
        part_send[k] = partial_rows(peer).astype(jnp.bfloat16)
        p_copies.append(remote(part_send.at[k], part_recv.at[k], ps.at[k], pr.at[k], "fs", peer))
    total = partial_rows(z)
    for copy in p_copies:
        copy.wait_recv()
    for k in range(1, N):
        total += part_recv[k].astype(jnp.float32)
    mixed_ref[...] = total.astype(jnp.bfloat16)

    for copy in (
        list(tok_copies.values()) + list(meta_copies.values()) + list(z_copies.values())
        + [c for _, c in y_copies] + x_copies + h_copies + p_copies
    ):
        copy.wait_send()


def on_device(G, N, T, tokens, route_ids, route_weights, ffn_gain, gate_master, up_master, down_master):
    experts, R, C = gate_master.shape
    R2, C2 = down_master.shape[1:]
    count, D = tokens.shape
    Ed = experts // N
    capacity = count // (2 * (experts // GROUP_SIZE))
    token_rows = tokens.astype(jnp.float32)
    normed = (
        token_rows * lax.rsqrt(jnp.mean(token_rows * token_rows, axis=1, keepdims=True) + 1e-06)
    ).astype(jnp.bfloat16)
    Dq = D // T
    quarters = normed.reshape(count, T, Dq).transpose(1, 0, 2)
    targets = slot_targets(route_ids, experts, capacity).reshape(count, 2)
    meta = jnp.concatenate(
        [targets.T.astype(jnp.float32), route_weights.T, jnp.zeros((4, count), jnp.float32)], axis=0
    )
    bf = jnp.bfloat16
    vmem = pl.BlockSpec(memory_space=pltpu.VMEM)
    anyspace = pl.BlockSpec(memory_space=pl.ANY)
    slots = N * capacity
    dma = pltpu.SemaphoreType.DMA
    return pl.pallas_call(
        functools.partial(kernel, G, N, T, capacity),
        out_shape=(
            jax.ShapeDtypeStruct((Ed, N * R, C), bf),
            jax.ShapeDtypeStruct((Ed, N * R, C), bf),
            jax.ShapeDtypeStruct((Ed, N * R2, C2), bf),
            jax.ShapeDtypeStruct((count, C2), bf),
        ),
        in_specs=[vmem, vmem, vmem, anyspace, anyspace, anyspace],
        out_specs=(vmem, vmem, vmem, vmem),
        scratch_shapes=[
            pltpu.VMEM((experts, R, C), jnp.float32),
            pltpu.VMEM((experts, R, C), jnp.float32),
            pltpu.VMEM((experts, R2, C2), jnp.float32),
            pltpu.VMEM((2, N, Ed, R // G, C), bf),
            pltpu.VMEM((N, Ed, R2 // G, C2), bf),
            pltpu.VMEM((N, T, count, Dq), bf),
            pltpu.VMEM((N, 8, count), jnp.float32),
            pltpu.VMEM((Ed, slots, D), bf),
            pltpu.VMEM((T, Ed, slots, C), bf),
            pltpu.VMEM((N, count, C2), bf),
            pltpu.VMEM((N, count, C2), bf),
            dma((3,)),
            dma((N,)), dma((N,)), dma((N,)), dma((N,)),
            dma((N, T)), dma((N, T)),
            dma((3, N)), dma((3, N)),
            dma((3, N, G)), dma((3, N, G)),
            dma((T,)), dma((T,)),
            dma((N,)), dma((N,)),
        ],
        compiler_params=pltpu.CompilerParams(
            collective_id=0, has_side_effects=True, vmem_limit_bytes=63 * 1024 * 1024
        ),
    )(quarters, meta, ffn_gain.reshape(R, 1), gate_master, up_master, down_master)


def solution(mesh):
    in_specs = (
        P(("grp", "fs"), None),
        P(("grp", "fs"), None),
        P(("grp", "fs"), None),
        P("fs"),
        P(None, "fs", "tp"),
        P(None, "fs", "tp"),
        P(None, "fs", "tp"),
    )
    out_specs = (
        P(("grp", "fs"), None, "tp"),
        P(("grp", "fs"), None, "tp"),
        P(("grp", "fs"), None, "tp"),
        P(("grp", "fs"), "tp"),
    )
    body = functools.partial(on_device, mesh.shape["grp"], mesh.shape["fs"], mesh.shape["tp"])
    return jax.shard_map(body, mesh=mesh, in_specs=in_specs, out_specs=out_specs, check_vma=False)
```

time: 251 us -> 166 us (0.66)
  the two profiles are of different devices: /device:TPU:0 before, /device:TPU:15 now
where the time goes in v1:
time: 166 us; the launch traced here: 165 us
  Pallas kernels  147 us (89%)
  local copies, waits for them, and re-layouts  13.5 us (8%)
  other arithmetic  3.85 us (2%)
    pallas_call x1, Pallas kernels, on_device(): pl.pallas_call(functools.partial(kernel, G, N, T, capacity), out_shape=(j...  147 us
    unnamed x12, local copies, waits for them, and re-layouts  9.85 us

profile of v1, /device:TPU:15, one launch (start us, length us, event | category | flops | bytes accessed | tf_op | source)
XLA Modules:
  0.0 165.4 jit_solution(10749805645295164988)
XLA Ops:
  0.6 0.1 pad.2.clone
  0.7 0.8 copy.13
  1.5 0.1 eq.29
  1.7 0.1 eq.25
  1.8 1.1 reduce-window.6
  3.0 0.2 slice_reduce_fusion
  3.2 0.1 fusion.3
  3.3 0.1 reduce_sum.22
  3.5 0.1 copy.15
  3.6 0.7 convert_bitcast_fusion
  4.3 1.3 maximum_maximum_fusion.meta_ref
  5.6 1.5 copy.16.gain_ref
  7.1 1.5 copy.11
  8.6 0.3 fusion
  8.9 0.2 fusion.1
  9.2 1.3 copy.12
  10.5 147.3 %shard_map.102 = (bf16[2,2048,256]{2,1,0:T(8,128)(2,1)}, bf16[2,2048,256]{2,1,0:T(8,128)(2,1)}, bf16[2,1024,512]{2,1,0:T(8,128)(2,1)}, bf16[256,512]{1,0:T(8,128)(2,1)}) custom-call(bf16[4,256,512]{2,1,0:T(8,128)(2,1)} %bitcast.14, f32[8,256]{1,0:T(8,128)} %maximum_maximum_fusion.meta_ref, f32[512,1]{1,0:T(8,128)} %copy.16.gain_ref, ...), custom_call_target="tpu_custom_call" | custom-call | tf_op jit(solution)/shard_map/pallas_call | solution.py:231
  157.8 0.0 copy-start.1
  157.8 3.2 %copy.21 = bf16[2,2048,256]{2,1,0:T(8,128)(2,1)} copy(bf16[2,2048,256]{2,1,0:T(8,128)(2,1)} %get-tuple-element.8) | data formatting | bytes 4194304
  161.0 0.0 copy-done.1
  161.0 1.3 copy.22
  162.4 1.0 copy-done
  163.4 1.3 copy.23
  164.7 0.7 copy.24
  (8 shorter events, 0.1 us)
Async XLA Ops:
  157.8 3.2 %copy-start.1 = (bf16[2,2048,256]{2,1,0:T(8,128)(2,1)S(1)}, bf16[2,2048,256]{2,1,0:T(8,128)(2,1)}, u32[]{:S(2)}) copy-start(bf16[2,2048,256]{2,1,0:T(8,128)(2,1)} %get-tuple-element.9) | copy-start | bytes 6291460
  161.0 2.3 %copy-start = (bf16[2,1024,512]{2,1,0:T(8,128)(2,1)S(1)}, bf16[2,1024,512]{2,1,0:T(8,128)(2,1)}, u32[]{:S(2)}) copy-start(bf16[2,1024,512]{2,1,0:T(8,128)(2,1)} %get-tuple-element.10) | copy-start | bytes 6291460
  163.4 1.3 copy-start.2

commit v2 on v0

v2 whole, which is shorter than its diff:
```python
import functools

import jax
import jax.numpy as jnp
from jax import lax
from jax.experimental import pallas as pl
from jax.experimental.pallas import tpu as pltpu
from jax.sharding import PartitionSpec as P

GROUP_SIZE = 8
MESH = pl.DeviceIdType.MESH


def kernel(
    G, N, T, cap,
    tok_ref, ids_ref, weights_ref, gain_ref, gate_hbm, up_hbm, down_hbm,
    gate_out, up_out, down_out, mixed_ref,
    gate_f, up_f, down_f, gs_ref, us_ref, ds_ref, gain_col, meta_ref, stage_gu, stage_d, tok_all, meta_all,
    x_buf, hid_all, ret_send, ret_recv, total_ref,
    load_sem, out_sem, ts, tr, ms, mr, xs, xr, zs, zr, ys, yr, hs, hr, ps, pr,
):
    g, z, t = lax.axis_index("grp"), lax.axis_index("fs"), lax.axis_index("tp")
    E, R, C = gate_f.shape
    Ed = E // N
    tokens, D = tok_ref.shape
    Dq = D // T
    masters, serves = (gate_f, up_f, down_f), (gs_ref, us_ref, ds_ref)
    outs = (gate_out, up_out, down_out)
    rows = (R, R, down_f.shape[1])

    loads = [
        pltpu.make_async_copy(src, dst, load_sem.at[w])
        for w, (src, dst) in enumerate(zip((gate_hbm, up_hbm, down_hbm), masters))
    ]
    for load in loads:
        load.start()

    barrier = pltpu.get_barrier_semaphore()
    for axis, me, size in (("grp", g, G), ("fs", z, N), ("tp", t, T)):
        for k in range(1, size):
            pl.semaphore_signal(barrier, inc=1, device_id={axis: lax.rem(me + k, size)}, device_id_type=MESH)

    def normalize(c, carry):
        at = pl.ds(pl.multiple_of(c * 32, 32), 32)
        wide = tok_ref[at, :].astype(jnp.float32)
        unit = (wide * lax.rsqrt(jnp.mean(wide * wide, axis=1, keepdims=True) + 1e-06)).astype(jnp.bfloat16)
        for q in range(T):
            tok_all[z, q, at, :] = unit[:, q * Dq:(q + 1) * Dq]
        return carry

    lax.fori_loop(0, tokens // 32, normalize, 0)

    expert_of = lax.broadcasted_iota(jnp.int32, (E, tokens), 0)
    named = [ids_ref[r:r + 1, :] == expert_of for r in range(2)]
    member = (named[0].astype(jnp.float32) + named[1].astype(jnp.float32)).astype(jnp.bfloat16)
    earlier = (
        lax.broadcasted_iota(jnp.int32, (tokens, tokens), 0) < lax.broadcasted_iota(jnp.int32, (tokens, tokens), 1)
    ).astype(jnp.float32).astype(jnp.bfloat16)
    place = jnp.dot(member, earlier, preferred_element_type=jnp.float32) + (expert_of * cap).astype(jnp.float32)
    meta_ref[...] = jnp.zeros_like(meta_ref)
    for r in range(2):
        meta_ref[r:r + 1, :] = jnp.sum(jnp.where(named[r], place, 0.0), axis=0, keepdims=True)
    meta_ref[2:4, :] = weights_ref[...]

    pl.semaphore_wait(barrier, G + N + T - 3)

    def describe(src, dst, send, recv, axis, peer):
        return pltpu.make_async_remote_copy(
            src_ref=src, dst_ref=dst, send_sem=send, recv_sem=recv, device_id={axis: peer}, device_id_type=MESH
        )

    def remote(*args):
        copy = describe(*args)
        copy.start()
        return copy

    def along(way):
        return z + (1 - 2 * way)

    def exists(way):
        return z < N - 1 if way == 0 else z > 0

    def reached(way, d):
        return z >= d if way == 0 else z + d < N

    def tok_step(way, d):
        origin = z - d if way == 0 else z + d
        view = tok_all.at[origin, t]
        return describe(view, view, ts.at[way, d], tr.at[way, d + 1], "fs", along(way))

    def tok_arrival(way, d):
        view = tok_all.at[z, t]
        return describe(view, view, ts.at[way, d - 1], tr.at[way, d], "fs", along(way))

    def tok_share(way, d, j):
        origin = z - d if way == 0 else z + d
        view = tok_all.at[origin, t]
        return describe(view, view, xs.at[way, d, j], xr.at[way, d, j], "tp", lax.rem(t + j, T))

    def each_way(d, condition, action):
        for way in range(2):
            pl.when(condition(way, d))(functools.partial(action, way, d))

    def can_pass(way, d):
        return exists(way) if d == 0 else jnp.logical_and(reached(way, d), exists(way))

    def pass_tokens(d):
        def arrive(way, d):
            tok_arrival(way, d).wait_recv()
            for j in range(1, T):
                tok_share(way, d, j).start()

        if d > 0:
            each_way(d, reached, arrive)
        if d < N - 1:
            each_way(d, can_pass, lambda way, d: tok_step(way, d).start())

    pass_tokens(0)
    meta_copies = {}
    for k in range(1, N):
        meta_copies[k] = remote(meta_ref, meta_all.at[z], ms.at[k], mr.at[k], "fs", lax.rem(z + k, N))

    square = (R, R)
    eye = lax.broadcasted_iota(jnp.int32, square, 0) == lax.broadcasted_iota(jnp.int32, square, 1)
    gain_col[...] = jnp.sum(jnp.where(eye, gain_ref[...], 0.0), axis=1, keepdims=True)

    z_copies = {}

    def send_weights(w, e):
        sub = rows[w] // G
        start = pl.multiple_of(g * sub, sub)
        where = pl.multiple_of(z * rows[w] + start, sub)
        for k in range(1, N):
            peer = lax.rem(z + k, N)
            stage = stage_d.at[e, k] if w == 2 else stage_gu.at[w, e, k]
            block = masters[w][peer * Ed + e, pl.ds(start, sub), :]
            if w < 2:
                block = block * gain_col[pl.ds(start, sub), :]
            stage[...] = block.astype(jnp.bfloat16)
            z_copies[w, e, k] = remote(
                stage, serves[w].at[e, pl.ds(where, sub), :], zs.at[w, e, k], zr.at[w, e, k], "fs", peer
            )

    def keep_own(w, e):
        where = pl.multiple_of(z * rows[w], rows[w])
        block = masters[w][z * Ed + e]
        if w < 2:
            block = block * gain_col[...]
        serves[w][e, pl.ds(where, rows[w]), :] = block.astype(jnp.bfloat16)

    y_copies, out_copies = {}, []

    def relay_weights(w, e):
        sub = rows[w] // G
        for k in range(1, N):
            z_copies[w, e, k].wait_recv()
            origin = lax.rem(z + N - k, N)
            where = pl.multiple_of(origin * rows[w] + g * sub, sub)
            view = serves[w].at[e, pl.ds(where, sub), :]
            for j in range(1, G):
                y_copies[w, e, k, j] = remote(
                    view, view, ys.at[w, e, k, j], yr.at[w, e, k, j], "grp", lax.rem(g + j, G)
                )

    def finish_weights(w, e):
        for k in range(1, N):
            for j in range(1, G):
                y_copies[w, e, k, j].wait_recv()
        copy = pltpu.make_async_copy(serves[w].at[e], outs[w].at[e], out_sem.at[w, e])
        copy.start()
        out_copies.append(copy)

    passed = 0
    for e in range(Ed):
        for w in range(3):
            if e == 0:
                loads[w].wait()
            send_weights(w, e)
            if passed < N - 1:
                passed += 1
                pass_tokens(passed)
    for d in range(passed + 1, N):
        pass_tokens(d)
    meta_all[z] = meta_ref[...]
    for e in range(Ed):
        for w in range(3):
            keep_own(w, e)
    for k in range(1, N):
        meta_copies[k].wait_recv()

    def hits(info, base):
        slot = lax.broadcasted_iota(jnp.int32, (cap, tokens), 0).astype(jnp.float32) + (base * cap).astype(jnp.float32)
        first, second = info[0:1, :] == slot, info[1:2, :] == slot
        return first, second, (first.astype(jnp.float32) + second.astype(jnp.float32)).astype(jnp.bfloat16)

    def dispatch(n, carry):
        info = meta_all[n]
        pick = jnp.concatenate([hits(info, z * Ed + e)[2].astype(jnp.float32) for e in range(Ed)], axis=0)
        pick = pick.astype(jnp.bfloat16)
        for q in range(T):
            got = jnp.dot(pick, tok_all[n, q], preferred_element_type=jnp.float32).astype(jnp.bfloat16)
            for e in range(Ed):
                x_buf[e, pl.ds(pl.multiple_of(n * cap, cap), cap), q * Dq:(q + 1) * Dq] = got[e * cap:(e + 1) * cap]
        return carry

    h_copies, p_copies = {}, {}

    def experts_in(e):
        def block(n, carry):
            at = pl.ds(pl.multiple_of(n * cap, cap), cap)
            x = x_buf[e, at, :]
            gate = jnp.dot(x, gs_ref[e], preferred_element_type=jnp.float32)
            up = jnp.dot(x, us_ref[e], preferred_element_type=jnp.float32)
            hid_all[t, e, at, :] = (gate / (1.0 + jnp.exp(-gate)) * up).astype(jnp.bfloat16)
            return carry

        lax.fori_loop(0, N, block, 0)
        view = hid_all.at[t, e]
        for j in range(1, T):
            h_copies[e, j] = remote(view, view, hs.at[e, j], hr.at[e, j], "tp", lax.rem(t + j, T))

    def experts_out(e):
        for j in range(1, T):
            h_copies[e, j].wait_recv()
        for k in list(range(1, N)) + [0]:
            peer = lax.rem(z + k, N)
            info = meta_all[peer]
            first, second, _ = hits(info, z * Ed + e)
            weight = jnp.sum(
                jnp.where(first, info[2:3, :], 0.0) + jnp.where(second, info[3:4, :], 0.0), axis=1, keepdims=True
            )
            at = pl.ds(pl.multiple_of(peer * cap, cap), cap)
            out = jnp.zeros((cap, ds_ref.shape[2]), jnp.float32)
            for q in range(T):
                out += jnp.dot(
                    hid_all[q, e, at, :], ds_ref[e, q * C:(q + 1) * C, :], preferred_element_type=jnp.float32
                )
            scaled = (out.astype(jnp.bfloat16).astype(jnp.float32) * weight).astype(jnp.bfloat16)
            if k == 0:
                ret_recv[e, 0] = scaled
            else:
                ret_send[e, k] = scaled
                p_copies[e, k] = remote(
                    ret_send.at[e, k], ret_recv.at[e, k], ps.at[e, k], pr.at[e, k], "fs", peer
                )

    def combine(e):
        info = meta_ref[...]
        for k in range(N):
            if k > 0:
                p_copies[e, k].wait_recv()
            pick = hits(info, lax.rem(z + N - k, N) * Ed + e)[2]
            part = lax.dot_general(
                pick, ret_recv[e, k], (((0,), (0,)), ((), ())), preferred_element_type=jnp.float32
            )
            if e == 0 and k == 0:
                total_ref[...] = part
            else:
                total_ref[...] += part

    for e in range(Ed):
        relay_weights(0, e)
        relay_weights(1, e)
        if e == 0:
            for d in range(1, N):
                each_way(d, reached, lambda way, d: [tok_share(way, d, j).wait_recv() for j in range(1, T)] and None)
            lax.fori_loop(0, N, dispatch, 0)
        finish_weights(0, e)
        finish_weights(1, e)
        experts_in(e)
        relay_weights(2, e)
        finish_weights(2, e)
        experts_out(e)
    for e in range(Ed):
        combine(e)
    mixed_ref[...] = total_ref[...].astype(jnp.bfloat16)

    for d in range(N - 1):
        each_way(d, can_pass, lambda way, d: tok_step(way, d).wait_send())
    for d in range(1, N):
        each_way(d, reached, lambda way, d: [tok_share(way, d, j).wait_send() for j in range(1, T)] and None)
    for group in (meta_copies, z_copies, y_copies, h_copies, p_copies):
        for copy in group.values():
            copy.wait_send()
    for copy in out_copies:
        copy.wait()


def on_device(G, N, T, tokens, route_ids, route_weights, ffn_gain, gate_master, up_master, down_master):
    experts, R, C = gate_master.shape
    R2, C2 = down_master.shape[1:]
    count, D = tokens.shape
    Ed = experts // N
    capacity = count // (2 * (experts // GROUP_SIZE))
    Dq = D // T
    bf = jnp.bfloat16
    vmem = pl.BlockSpec(memory_space=pltpu.VMEM)
    anyspace = pl.BlockSpec(memory_space=pl.ANY)
    slots = N * capacity
    dma = pltpu.SemaphoreType.DMA
    return pl.pallas_call(
        functools.partial(kernel, G, N, T, capacity),
        out_shape=(
            jax.ShapeDtypeStruct((Ed, N * R, C), bf),
            jax.ShapeDtypeStruct((Ed, N * R, C), bf),
            jax.ShapeDtypeStruct((Ed, N * R2, C2), bf),
            jax.ShapeDtypeStruct((count, C2), bf),
        ),
        in_specs=[vmem, vmem, vmem, vmem, anyspace, anyspace, anyspace],
        out_specs=(anyspace, anyspace, anyspace, vmem),
        scratch_shapes=[
            pltpu.VMEM((experts, R, C), jnp.float32),
            pltpu.VMEM((experts, R, C), jnp.float32),
            pltpu.VMEM((experts, R2, C2), jnp.float32),
            pltpu.VMEM((Ed, N * R, C), bf),
            pltpu.VMEM((Ed, N * R, C), bf),
            pltpu.VMEM((Ed, N * R2, C2), bf),
            pltpu.VMEM((R, 1), jnp.float32),
            pltpu.VMEM((8, count), jnp.float32),
            pltpu.VMEM((2, Ed, N, R // G, C), bf),
            pltpu.VMEM((Ed, N, R2 // G, C2), bf),
            pltpu.VMEM((N, T, count, Dq), bf),
            pltpu.VMEM((N, 8, count), jnp.float32),
            pltpu.VMEM((Ed, slots, D), bf),
            pltpu.VMEM((T, Ed, slots, C), bf),
            pltpu.VMEM((Ed, N, capacity, C2), bf),
            pltpu.VMEM((Ed, N, capacity, C2), bf),
            pltpu.VMEM((count, C2), jnp.float32),
            dma((3,)), dma((3, Ed)),
            dma((2, N)), dma((2, N)), dma((N,)), dma((N,)),
            dma((2, N, T)), dma((2, N, T)),
            dma((3, Ed, N)), dma((3, Ed, N)),
            dma((3, Ed, N, G)), dma((3, Ed, N, G)),
            dma((Ed, T)), dma((Ed, T)),
            dma((Ed, N)), dma((Ed, N)),
        ],
        compiler_params=pltpu.CompilerParams(
            collective_id=0, has_side_effects=True, vmem_limit_bytes=63 * 1024 * 1024
        ),
    )(tokens, route_ids.T, route_weights.T, ffn_gain.reshape(1, R), gate_master, up_master, down_master)


def solution(mesh):
    in_specs = (
        P(("grp", "fs"), None),
        P(("grp", "fs"), None),
        P(("grp", "fs"), None),
        P("fs"),
        P(None, "fs", "tp"),
        P(None, "fs", "tp"),
        P(None, "fs", "tp"),
    )
    out_specs = (
        P(("grp", "fs"), None, "tp"),
        P(("grp", "fs"), None, "tp"),
        P(("grp", "fs"), None, "tp"),
        P(("grp", "fs"), "tp"),
    )
    body = functools.partial(on_device, mesh.shape["grp"], mesh.shape["fs"], mesh.shape["tp"])
    return jax.shard_map(body, mesh=mesh, in_specs=in_specs, out_specs=out_specs, check_vma=False)
```

time: 251 us -> 137 us (0.55)
  waiting for transfers between devices: 171 us -> 0 us
  Pallas kernels: 0 us -> 127 us
  starting transfers between devices: 21.8 us -> 0 us
  other arithmetic: 15.5 us -> 0 us
  between operations: 14.3 us -> 0.65 us
  local copies, waits for them, and re-layouts: 17.5 us -> 7.57 us
  matrix products: 9.85 us -> 0 us
    all_to_all x5 -> x0, waiting for transfers between devices: 171 us -> none  [the longest x1 46.5 us: on_device(): lax.all_to_all(gate_local, 'fs', split_axis=0, concat_axis=1, tiled=True)]
    pallas_call x0 -> x1, Pallas kernels: none -> 127 us  [on_device(): pl.pallas_call(functools.partial(kernel, G, N, T, capacity), out_shape=(j...]
    all_to_all x5 -> x0, starting transfers between devices: 21.7 us -> none  [the longest x1 6.35 us: on_device(): lax.all_to_all(fill_slots(own_cols, targets, experts, capacity), 'fs', sp...]
    convert_element_type x5 -> x0, other arithmetic: 11.9 us -> none  [the longest x1 6.46 us: on_device(): up_local = (up_master * row_gain).astype(jnp.bfloat16)]
    dot_general x3 -> x0, matrix products: 9.85 us -> none  [the longest x1 4.25 us: on_device(): jnp.einsum('erd,edf->erf', portion, gate_serve, preferred_element_type=jn...]
    all_to_all x5 -> x0, local copies, waits for them, and re-layouts: 7.4 us -> none  [the longest x1 3.05 us: on_device(): lax.all_to_all(up_local, 'fs', split_axis=0, concat_axis=1, tiled=True)]
    unnamed x14 -> x10, local copies, waits for them, and re-layouts: 0.71 us -> 7.57 us
    scatter x1 -> x0, local copies, waits for them, and re-layouts: 3.47 us -> none  [fill_slots(): jnp.zeros((experts * capacity, source.shape[1]), source.dtype).at[targets]]
  transfers between devices with their start and end apart: 7 -> 0, of which waited for: 5 -> 0; matrix products, arithmetic and copies ran while one was open for 10% -> 0% of each run, Pallas kernels for 0% -> 0%
where the time goes in v2:
time: 137 us; the launch traced here: 136 us
  Pallas kernels  127 us (93%)
  local copies, waits for them, and re-layouts  7.57 us (6%)
    pallas_call x1, Pallas kernels, on_device(): pl.pallas_call(functools.partial(kernel, G, N, T, capacity), out_shape=(j...  127 us
    unnamed x10, local copies, waits for them, and re-layouts  7.57 us

profile of v2, /device:TPU:0, one launch (start us, length us, event | category | flops | bytes accessed | tf_op | source)
XLA Modules:
  0.0 135.7 jit_solution(14570380521630672736)
XLA Ops:
  0.6 127.5 %shard_map.102 = (bf16[2,2048,256]{2,1,0:T(8,128)(2,1)}, bf16[2,2048,256]{2,1,0:T(8,128)(2,1)}, bf16[2,1024,512]{2,1,0:T(8,128)(2,1)}, bf16[256,512]{1,0:T(8,128)(2,1)}) custom-call(bf16[256,2048]{1,0:T(8,128)(2,1)} %tok_ref.1, s32[2,256]{1,0:T(2,128)} %bitcast.3, f32[2,256]{1,0:T(2,128)} %bitcast.4, f32[1,512]{1,0:T(1,128)} %bitcast.5, ...), custom_call_target="tpu_custom_call" | custom-call | tf_op jit(solution)/shard_map/pallas_call | solution.py:301
  128.1 0.0 copy-start.1
  128.1 3.2 %copy.15 = bf16[2,2048,256]{2,1,0:T(8,128)(2,1)} copy(bf16[2,2048,256]{2,1,0:T(8,128)(2,1)} %get-tuple-element.8) | data formatting | bytes 4194304
  131.3 0.0 copy-done.1
  131.3 0.0 copy-start
  131.3 1.3 copy.16
  132.7 1.0 copy-done
  133.7 0.0 copy-start.2
  133.7 1.3 copy.17
  135.0 0.0 copy-done.2
  135.0 0.7 copy.18
Async XLA Ops:
  128.1 3.2 %copy-start.1 = (bf16[2,2048,256]{2,1,0:T(8,128)(2,1)S(1)}, bf16[2,2048,256]{2,1,0:T(8,128)(2,1)}, u32[]{:S(2)}) copy-start(bf16[2,2048,256]{2,1,0:T(8,128)(2,1)} %get-tuple-element.9) | copy-start | bytes 6291460
  131.3 2.3 %copy-start = (bf16[2,1024,512]{2,1,0:T(8,128)(2,1)S(1)}, bf16[2,1024,512]{2,1,0:T(8,128)(2,1)}, u32[]{:S(2)}) copy-start(bf16[2,1024,512]{2,1,0:T(8,128)(2,1)} %get-tuple-element.10) | copy-start | bytes 6291460
  133.7 1.3 copy-start.2
